TPU v7x, 512 devices: a whole 4x8x8 slice. The times are simulated.
512 devices in a mesh: sp: 32 (over z, x), tp: 16 (over y, core).
Axes of the slice: x: 4, y: 8, z: 8, core: 2. Of those that a mesh axis runs over, the one named last changes fastest.
Arguments:
- lane_source_signal: bfloat16 [1024, 4096], P('tp', 'sp'), may hold values from -6 to 6
- spectral_damping_part: float32 [64, 64], P('tp'), may hold values from -3 to -0.0002
- spectral_angular_part: float32 [64, 64], P('tp'), may hold values from 0.31 to 201.0624
- interval_exponent: float32 [64], P('tp'), may hold values from -3.9 to -1.6
- entry_matrix_inphase: float32 [64, 64, 16], P('tp'), may hold values from -1 to 1
- entry_matrix_quadrature: float32 [64, 64, 16], P('tp'), may hold values from -1 to 1
- emission_inphase: float32 [64, 16, 64], P('tp'), may hold values from -0.75 to 0.75
- emission_quadrature: float32 [64, 16, 64], P('tp'), may hold values from -0.75 to 0.75
- lane_bypass_factor: float32 [1024], P('tp'), may hold values from -5 to 5
- spike_shrink_offset: float32 [64, 4096], P('tp', 'sp'), may hold values from -1.4 to 0
- lane_exit_matrix: bfloat16 [1024, 4096], P('tp'), may hold values from -0.1875 to 0.1875
- skipline_stream: bfloat16 [4096, 4096], P('sp'), may hold values from -6 to 6
- specialist_scaling_vector: float32 [4096], replicated, may hold values from 0.1 to 1.9
- selected_specialists: int32 [4096, 2], P('sp'), may hold values from 0 to 31, all different within a row; in each aligned block of 128 rows (0 to 127, 128 to 255, ...) at most 16 rows name the same one
- dispatcher_scores: float32 [4096, 2], P('sp'), may hold values from 0.1 to 1
- specialist_valve_matrix: bfloat16 [32, 4096, 2048], P('sp', None, 'tp'), may hold values from -0.09375 to 0.09375
- specialist_widen_matrix: bfloat16 [32, 4096, 2048], P('sp', None, 'tp'), may hold values from -0.09375 to 0.09375
- specialist_shrink_matrix: bfloat16 [32, 2048, 4096], P('sp', 'tp'), may hold values from -0.1875 to 0.1875
Outputs:
- updated: bfloat16 [4096, 4096], P('sp', 'tp')
Inputs may be any that keep to these rules, and one draw needn't show every extreme that they name: `selected_specialists`: each row names 2 different experts. Among the rows of each aligned block of 128 positions no expert is named more than 16 times, and in every block some expert is named exactly 16 times.
All inputs are finite; a program needn't handle non-finite values.
Results may differ from a plain program's by a relative error of at most 0.019.
Values may be sent and summed in bfloat16 or wider, within the bound.
A program may use at most 64 MiB of HBM per device.

v0:
```python
import jax
import jax.numpy as jnp
from jax import lax
from jax.sharding import PartitionSpec as P

EPS = 1e-06
PRECISE_MODE = lax.Precision.HIGHEST


def copy_for_each(array, axis):
    copies = jnp.broadcast_to(array, (lax.axis_size(axis), *array.shape))
    return lax.all_to_all(copies, axis, split_axis=0, concat_axis=0, tiled=True)


def gathered_once(array, axis):
    leaves = jax.tree.leaves(array)
    order = sorted(range(len(leaves)), key=lambda k: -leaves[k].size)
    width = (1, *leaves[order[0]].shape)[-1]
    lines = [
        jnp.pad(leaves[k].reshape(-1), (0, -leaves[k].size % width)).reshape(-1, width)
        for k in order
    ]
    both, at, found = (copy_for_each(jnp.concatenate(lines), axis), 0, {})
    for k, line in zip(order, lines):
        share = both[:, at : at + len(line)].reshape(len(both), -1)
        found[k] = share[:, : leaves[k].size].reshape(-1, *leaves[k].shape)
        at += len(line)
    numbers = iter(range(len(leaves)))
    return jax.tree.map(lambda _: found[next(numbers)], array)


def combined_pairwise(pieces, combine):
    while len(jax.tree.leaves(pieces)[0]) > 1:
        pieces = jax.vmap(combine)(
            *(jax.tree.map(lambda part: part[side::2], pieces) for side in (0, 1))
        )
    return jax.tree.map(lambda part: part[0], pieces)


def prefix(array, axis, combine, identity):
    length, mine = (lax.axis_size(axis), lax.axis_index(axis))
    passed = jnp.arange(length) < mine

    def kept(part, zero, own):
        part = jnp.where(
            passed.reshape(-1, *(1 for _ in own.shape)), part, jnp.asarray(zero, own.dtype)
        )
        return part

    pieces = gathered_once(array, axis)
    return combined_pairwise(jax.tree.map(kept, pieces, identity, array), combine)


def in_blocks(array, dim, length):
    before, after = (array.shape[:dim], array.shape[dim + 1 :])
    return jnp.moveaxis(array.reshape(*before, length, -1, *after), dim, 0)


def sent_and_summed(array, axis, dim):
    length = lax.axis_size(axis)
    parts = lax.all_to_all(in_blocks(array, dim, length), axis, 0, 0, tiled=True)
    return jnp.sum(parts.astype(jnp.float32), axis=0)


def taken_together(array, axis):
    return copy_for_each(array, axis).sum(axis=0)


def affine_pair(earlier, latter):
    mul_re = earlier[0] * latter[0] - earlier[1] * latter[1]
    mul_im = earlier[0] * latter[1] + earlier[1] * latter[0]
    add_re = latter[0] * earlier[2] - latter[1] * earlier[3] + latter[2]
    add_im = latter[0] * earlier[3] + latter[1] * earlier[2] + latter[3]
    return (mul_re, mul_im, add_re, add_im)


def local_prefix(elements):
    length = elements[0].shape[2]
    fills = (1.0, 0.0, 0.0, 0.0)
    offset = 1
    while offset < length:
        earlier = tuple(
            (
                jnp.pad(
                    item[:, :, : length - offset],
                    ((0, 0), (0, 0), (offset, 0)),
                    constant_values=fill,
                )
                for item, fill in zip(elements, fills)
            )
        )
        elements = affine_pair(earlier, elements)
        offset = offset * 2
    return elements


def per_device(
    lane_source_signal,
    spectral_damping_part,
    spectral_angular_part,
    interval_exponent,
    entry_matrix_inphase,
    entry_matrix_quadrature,
    emission_inphase,
    emission_quadrature,
    lane_bypass_factor,
    spike_shrink_offset,
    lane_exit_matrix,
    skipline_stream,
    specialist_scaling_vector,
    selected_specialists,
    dispatcher_scores,
    specialist_valve_matrix,
    specialist_widen_matrix,
    specialist_shrink_matrix,
):
    f32 = jnp.float32
    bf16 = jnp.bfloat16
    groups_here = spectral_damping_part.shape[0]
    lanes_within_bundle = entry_matrix_inphase.shape[2]
    tok_local = lane_source_signal.shape[1]
    bundled_signal = lane_source_signal.astype(f32).reshape(
        groups_here, lanes_within_bundle, tok_local
    )
    step_size = jnp.exp(interval_exponent)[:, None]
    natural_pace_exponent = spectral_damping_part * step_size
    angle = spectral_angular_part * step_size
    num_re = jnp.expm1(natural_pace_exponent) * jnp.cos(angle) - 2.0 * jnp.sin(0.5 * angle) ** 2
    num_im = jnp.exp(natural_pace_exponent) * jnp.sin(angle)
    denom = (
        spectral_damping_part * spectral_damping_part
        + spectral_angular_part * spectral_angular_part
    )
    fac_re = (num_re * spectral_damping_part + num_im * spectral_angular_part) / denom
    fac_im = (num_im * spectral_damping_part - num_re * spectral_angular_part) / denom
    map_re = (
        fac_re[:, :, None] * entry_matrix_inphase - fac_im[:, :, None] * entry_matrix_quadrature
    )
    map_im = (
        fac_re[:, :, None] * entry_matrix_quadrature + fac_im[:, :, None] * entry_matrix_inphase
    )
    drive_re = jnp.einsum("gpc,gct->gpt", map_re, bundled_signal, precision=PRECISE_MODE)
    drive_im = jnp.einsum("gpc,gct->gpt", map_im, bundled_signal, precision=PRECISE_MODE)
    recurrence_modulus = jnp.exp(
        natural_pace_exponent[:, :, None] + spike_shrink_offset[:, None, :]
    )
    trans_re = recurrence_modulus * jnp.cos(angle)[:, :, None]
    trans_im = recurrence_modulus * jnp.sin(angle)[:, :, None]
    cum_re, cum_im, state_real, state_imaginary = local_prefix(
        (trans_re, trans_im, drive_re, drive_im)
    )
    summary = (cum_re[:, :, -1], cum_im[:, :, -1], state_real[:, :, -1], state_imaginary[:, :, -1])
    unit = jnp.ones_like(summary[0])
    blank = jnp.zeros_like(summary[0])
    carried = prefix(summary, "sp", affine_pair, (unit, blank, blank, blank))
    enter_re = carried[2][:, :, None]
    enter_im = carried[3][:, :, None]
    state_real = state_real + cum_re * enter_re - cum_im * enter_im
    state_imaginary = state_imaginary + cum_re * enter_im + cum_im * enter_re
    value = (
        jnp.einsum("nef,nfi->nei", emission_inphase, state_real, precision=PRECISE_MODE)
        - jnp.einsum("nef,nfi->nei", emission_quadrature, state_imaginary, precision=PRECISE_MODE)
        + lane_bypass_factor.reshape(groups_here, lanes_within_bundle)[:, :, None] * bundled_signal
    )
    recurrence_result = (
        jax.nn.gelu(value).astype(bf16).reshape(groups_here * lanes_within_bundle, tok_local)
    )
    width = specialist_scaling_vector.shape[0]
    d_local = width // lax.axis_size("tp")
    col_start = lax.axis_index("tp") * d_local
    partial_rows = jnp.einsum(
        "ct,cd->td", recurrence_result, lane_exit_matrix, preferred_element_type=f32
    )
    projected_own = sent_and_summed(partial_rows.astype(jnp.bfloat16), "tp", 1).astype(bf16)
    own_residual = lax.dynamic_slice_in_dim(skipline_stream, col_start, d_local, 1)
    stream_own = (
        own_residual.astype(f32) + lax.optimization_barrier(projected_own).astype(f32)
    ).astype(bf16)
    own_stream = lax.optimization_barrier(stream_own).astype(f32)
    square_total = taken_together(jnp.sum(own_stream * own_stream, axis=1), "tp")
    inv_rms = lax.rsqrt(square_total / width + EPS)[:, None]
    own_gain = lax.dynamic_slice_in_dim(specialist_scaling_vector, col_start, d_local, 0)
    own_cols = (own_stream * inv_rms * own_gain).astype(bf16)
    share = dispatcher_scores / jnp.sum(dispatcher_scores, axis=1, keepdims=True)
    experts = lax.axis_size("sp")
    top = selected_specialists.shape[1]
    capacity = 2 * tok_local * top // experts
    flat_routes = selected_specialists.reshape(-1)
    hits = (flat_routes[:, None] == jnp.arange(experts, dtype=jnp.int32)[None, :]).astype(jnp.int32)
    ranks = jnp.sum((jnp.cumsum(hits, axis=0) - hits) * hits, axis=1)
    slot_ids = flat_routes * capacity + ranks
    slot_grid = jnp.arange(experts * capacity, dtype=jnp.int32)
    matched = slot_grid[:, None] == slot_ids[None, :]
    token_of = jnp.arange(tok_local * top, dtype=jnp.int32) // top
    slot_token = jnp.sum(jnp.where(matched, token_of[None, :], 0), axis=1)
    slot_live = jnp.any(matched, axis=1)
    gate_w = specialist_valve_matrix[0]
    up_w = specialist_widen_matrix[0]
    down_w = specialist_shrink_matrix[0]
    bf_zero = jnp.zeros((), bf16)
    dispatch = jnp.where(slot_live[:, None], own_cols[slot_token], bf_zero).reshape(
        experts, capacity, d_local
    )
    arrived = lax.all_to_all(dispatch, "sp", split_axis=0, concat_axis=0, tiled=True)
    piece = lax.all_gather(arrived, "tp", axis=2, tiled=True)
    gate_part = jnp.einsum("snd,df->snf", piece, gate_w, preferred_element_type=f32)
    up_part = jnp.einsum("snd,df->snf", piece, up_w, preferred_element_type=f32)
    hidden = (jax.nn.silu(gate_part) * up_part).astype(bf16)
    flat_hidden = hidden.reshape(experts * capacity, hidden.shape[2])
    down_part = jnp.dot(flat_hidden, down_w, preferred_element_type=f32).astype(bf16)
    summed = lax.psum_scatter(
        down_part.astype(f32).astype(jnp.bfloat16), "tp", scatter_dimension=1, tiled=True
    ).astype(jnp.float32)
    expert_out = summed.astype(bf16).reshape(experts, capacity, d_local)
    returned = lax.all_to_all(expert_out, "sp", split_axis=0, concat_axis=0, tiled=True).reshape(
        experts * capacity, d_local
    )
    picked = returned[slot_ids].reshape(tok_local, top, d_local)
    combined = jnp.sum(lax.optimization_barrier(picked).astype(f32) * share[:, :, None], axis=1)
    return (own_stream + combined).astype(bf16)


def solution(mesh):
    placed = (
        P("tp", "sp"),
        P("tp", None),
        P("tp", None),
        P("tp"),
        P("tp", None, None),
        P("tp", None, None),
        P("tp", None, None),
        P("tp", None, None),
        P("tp"),
        P("tp", "sp"),
        P("tp", None),
        P("sp", None),
        P(),
        P("sp", None),
        P("sp", None),
        P("sp", None, "tp"),
        P("sp", None, "tp"),
        P("sp", "tp", None),
    )
    return jax.shard_map(
        per_device, mesh=mesh, in_specs=placed, out_specs=P("sp", "tp"), check_vma=False
    )
```

profile of v0, /device:TPU:25, one launch (start us, length us, event | category | flops | bytes accessed | tf_op | source)
XLA Modules:
  0.0 256.6 jit_solution(5773878891755166815)
XLA Ops:
  6.5 0.7 exp.13
  7.3 0.8 fusion.57
  8.1 1.1 fusion.42
  9.2 1.1 fusion.46
  10.3 0.9 subtract_add_fusion.6
  11.2 1.0 add_add_fusion.5
  12.3 0.2 add_add_fusion.4
  12.7 0.2 add_add_fusion.3
  13.1 0.2 add_add_fusion.2
  13.4 0.2 add_add_fusion.1
  13.8 0.2 add_add_fusion
  14.0 0.2 multiply_subtract_fusion
  14.2 0.3 slice_reduce_fusion.1
  14.5 0.3 slice_reduce_fusion
  14.8 0.8 reshape.198
  15.6 12.9 %all-to-all-start = ((f32[32,1,1024]{2,1,0:T(1,128)}), f32[32,1,1024]{2,1,0:T(1,128)S(1)}, u32[]{:S(2)}, u32[]{:S(2)}) async-start(f32[32,1,1024]{2,1,0:T(1,128)} %reshape.198), calls=%async_computation | async-start | bytes 262144 | tf_op jit(solution)/shard_map/all_to_all | solution.py:12
  28.6 9.2 %all-to-all-done = f32[32,1,1024]{2,1,0:T(1,128)S(1)} async-done(((f32[32,1,1024]{2,1,0:T(1,128)}), f32[32,1,1024]{2,1,0:T(1,128)S(1)}, u32[]{:S(2)}, u32[]{:S(2)}) %all-to-all-start) | async-done | bytes 131104 | tf_op jit(solution)/shard_map/all_to_all | solution.py:12
  37.9 0.5 broadcast.191
  38.4 0.9 reduce.12
  39.7 0.3 fusion.16
  40.1 0.4 fusion.36
  40.5 0.4 convolution_convert_fusion.1
  40.9 1.1 copy.117
  42.0 9.1 %all-to-all-start.1 = ((bf16[16,128,256]{2,1,0:T(8,128)(2,1)}), bf16[16,128,256]{2,1,0:T(8,128)(2,1)S(1)}, u32[]{:S(2)}, u32[]{:S(2)}) async-start(bf16[16,128,256]{2,1,0:T(8,128)(2,1)} %bitcast.68), calls=%async_computation.1 | async-start | bytes 2097152 | tf_op jit(solution)/shard_map/all_to_all | solution.py:61
  51.4 0.1 reshape.168
  51.6 0.6 reduce-window.6
  52.2 0.2 slice_reduce_fusion.4
  52.5 0.2 fusion.7
  52.7 0.2 select_reduce_fusion
  52.9 24.5 %all-to-all-done.1 = bf16[16,128,256]{2,1,0:T(8,128)(2,1)S(1)} async-done(((bf16[16,128,256]{2,1,0:T(8,128)(2,1)}), bf16[16,128,256]{2,1,0:T(8,128)(2,1)S(1)}, u32[]{:S(2)}, u32[]{:S(2)}) %all-to-all-start.1) | async-done | bytes 1048608 | tf_op jit(solution)/shard_map/all_to_all | solution.py:61
  77.4 0.1 reduce_sum.70
  77.5 0.9 add_convert_fusion
  78.5 0.6 broadcast_in_dim.86
  79.1 5.2 %all-to-all-start.2 = ((f32[16,1,128]{2,1,0:T(1,128)}), f32[16,1,128]{2,1,0:T(1,128)S(1)}, u32[]{:S(2)}, u32[]{:S(2)}) async-start(f32[16,1,128]{2,1,0:T(1,128)} %broadcast_in_dim.86), calls=%async_computation.2 | async-start | bytes 16384 | tf_op jit(solution)/shard_map/all_to_all | solution.py:12
  84.4 0.8 dynamic_slice.7
  85.3 3.2 %all-to-all-done.2 = f32[16,1,128]{2,1,0:T(1,128)S(1)} async-done(((f32[16,1,128]{2,1,0:T(1,128)}), f32[16,1,128]{2,1,0:T(1,128)S(1)}, u32[]{:S(2)}, u32[]{:S(2)}) %all-to-all-start.2) | async-done | bytes 8224 | tf_op jit(solution)/shard_map/all_to_all | solution.py:12
  88.6 2.0 gather_fusion
  90.7 15.2 %all_to_all.26 = bf16[32,16,256]{2,1,0:T(8,128)(2,1)} all-to-all(bf16[32,16,256]{2,1,0:T(8,128)(2,1)S(1)} %broadcast_select_fusion), channel_id=1, replica_groups=mesh['sp'=32,'tp'=16] {'sp'}, dimensions={0} | all-to-all | bytes 524288 | tf_op jit(solution)/shard_map/all_to_all | solution.py:204
  106.0 45.2 %all-gather.2.cloned.1.call-done = bf16[32,16,4096]{2,1,0:T(8,128)(2,1)} async-done(((bf16[32,16,256]{2,1,0:T(8,128)(2,1)}), bf16[32,16,4096]{2,1,0:T(8,128)(2,1)}) %all-gather.2.cloned.1.call-update) | async-done | bytes 4194320 | tf_op jit(solution)/shard_map/all_gather | solution.py:205
  151.2 3.6 %fusion.5 = f32[32,16,128]{2,1,0:T(8,128)S(1)} fusion(bf16[32,16,4096]{2,1,0:T(8,128)(2,1)} %all-gather.2.cloned.1.call-done, bf16[1,4096,128]{2,1,0:T(8,128)(2,1)S(1)} %copy-done.2), kind=kOutput, calls=%fused_computation.12 | convolution fusion | flops 536870912 | bytes 5505024 | tf_op jit(solution)/shard_map/snd,df->snf/dot_general | solution.py:206
  154.8 2.5 fusion
  157.3 3.2 %convolution_convert_fusion = bf16[512,4096]{1,0:T(8,128)(2,1)} fusion(bf16[512,128]{1,0:T(8,128)(2,1)S(1)} %bitcast.140, bf16[1,128,4096]{2,1,0:T(8,128)(2,1)S(1)} %copy-done), kind=kOutput, calls=%fused_computation.2 | convolution fusion | flops 538968064 | bytes 5373952 | tf_op jit(solution)/shard_map/dot_general | solution.py:210
  160.8 65.8 %reduce-scatter.2.cloned.1.call-done = bf16[512,256]{1,0:T(8,128)(2,1)} async-done(((bf16[512,4096]{1,0:T(8,128)(2,1)}), bf16[512,256]{1,0:T(8,128)(2,1)}) %reduce-scatter.2.cloned.1.call-update) | async-done | bytes 262160 | tf_op jit(solution)/shard_map/reduce_scatter | solution.py:211
  226.6 9.7 %all-to-all-start.4 = ((bf16[32,16,256]{2,1,0:T(8,128)(2,1)}), bf16[32,16,256]{2,1,0:T(8,128)(2,1)S(1)}, u32[]{:S(2)}, u32[]{:S(2)}) async-start(bf16[32,16,256]{2,1,0:T(8,128)(2,1)} %bitcast.141), calls=%async_computation.5 | async-start | bytes 524288 | tf_op jit(solution)/shard_map/all_to_all | solution.py:215
  236.5 11.0 %all-to-all-done.4 = bf16[32,16,256]{2,1,0:T(8,128)(2,1)S(1)} async-done(((bf16[32,16,256]{2,1,0:T(8,128)(2,1)}), bf16[32,16,256]{2,1,0:T(8,128)(2,1)S(1)}, u32[]{:S(2)}, u32[]{:S(2)}) %all-to-all-start.4) | async-done | bytes 262176 | tf_op jit(solution)/shard_map/all_to_all | solution.py:215
  247.5 1.2 gather_fusion.1
  248.7 0.4 multiply_reduce_fusion
  249.1 0.6 fusion.11
  (65 shorter events, 2.6 us)
Async XLA Ops:
  6.5 150.8 %copy-start = (bf16[1,128,4096]{2,1,0:T(8,128)(2,1)S(1)}, bf16[1,128,4096]{2,1,0:T(8,128)(2,1)}, u32[]{:S(2)}) copy-start(bf16[1,128,4096]{2,1,0:T(8,128)(2,1)} %param.35) | copy-start | bytes 3145732
  13.0 15.5 %copy-start.9 = (f32[64]{0:T(128)S(1)}, f32[64]{0:T(128)}, u32[]{:S(2)}) copy-start(f32[64]{0:T(128)} %param.26) | copy-start | bytes 772
  13.4 26.3 %copy-start.5 = (f32[4,16,64]{2,1,0:T(8,128)S(1)}, f32[4,16,64]{2,1,0:T(8,128)}, u32[]{:S(2)}) copy-start(f32[4,16,64]{2,1,0:T(8,128)} %param.24) | copy-start | bytes 49156
  13.4 26.7 %copy-start.4 = (bf16[64,128]{1,0:T(8,128)(2,1)S(1)}, bf16[64,128]{1,0:T(8,128)(2,1)}, u32[]{:S(2)}) copy-start(bf16[64,128]{1,0:T(8,128)(2,1)} %param.18) | copy-start | bytes 49156
  13.4 26.7 %copy-start.6 = (f32[4,16,64]{2,1,0:T(8,128)S(1)}, f32[4,16,64]{2,1,0:T(8,128)}, u32[]{:S(2)}) copy-start(f32[4,16,64]{2,1,0:T(8,128)} %param.25) | copy-start | bytes 49156
  13.7 26.8 %copy-start.3 = (bf16[64,4096]{1,0:T(8,128)(2,1)S(1)}, bf16[64,4096]{1,0:T(8,128)(2,1)}, u32[]{:S(2)}) copy-start(bf16[64,4096]{1,0:T(8,128)(2,1)} %param.28) | copy-start | bytes 1572868
  15.6 22.2 %all-to-all-start = ((f32[32,1,1024]{2,1,0:T(1,128)}), f32[32,1,1024]{2,1,0:T(1,128)S(1)}, u32[]{:S(2)}, u32[]{:S(2)}) async-start(f32[32,1,1024]{2,1,0:T(1,128)} %reshape.198), calls=%async_computation | async-start | bytes 262144 | tf_op jit(solution)/shard_map/all_to_all | solution.py:12
  39.3 11.8 %copy-start.7 = (s32[128,2]{0,1:T(2,128)S(1)}, s32[128,2]{0,1:T(2,128)}, u32[]{:S(2)}) copy-start(s32[128,2]{0,1:T(2,128)} %param.31) | copy-start | bytes 3076
  42.0 109.2 %copy-start.2 = (bf16[1,4096,128]{2,1,0:T(8,128)(2,1)S(1)}, bf16[1,4096,128]{2,1,0:T(8,128)(2,1)}, u32[]{:S(2)}) copy-start(bf16[1,4096,128]{2,1,0:T(8,128)(2,1)} %param.33) | copy-start | bytes 3145732
  42.0 35.3 %all-to-all-start.1 = ((bf16[16,128,256]{2,1,0:T(8,128)(2,1)}), bf16[16,128,256]{2,1,0:T(8,128)(2,1)S(1)}, u32[]{:S(2)}, u32[]{:S(2)}) async-start(bf16[16,128,256]{2,1,0:T(8,128)(2,1)} %bitcast.68), calls=%async_computation.1 | async-start | bytes 2097152 | tf_op jit(solution)/shard_map/all_to_all | solution.py:61
  79.1 9.3 %all-to-all-start.2 = ((f32[16,1,128]{2,1,0:T(1,128)}), f32[16,1,128]{2,1,0:T(1,128)S(1)}, u32[]{:S(2)}, u32[]{:S(2)}) async-start(f32[16,1,128]{2,1,0:T(1,128)} %broadcast_in_dim.86), calls=%async_computation.2 | async-start | bytes 16384 | tf_op jit(solution)/shard_map/all_to_all | solution.py:12
  84.4 66.9 %all-gather.2.cloned.1.call-start = ((), (), s32[]{:S(2)}) async-start(), calls=%async_computation.6 | async-start | bytes 4456448 | tf_op jit(solution)/shard_map/all_gather | solution.py:205
  105.9 120.7 %reduce-scatter.2.cloned.1.call-start = ((), (), s32[]{:S(2)}) async-start(), calls=%async_computation.7 | async-start | bytes 4456448 | tf_op jit(solution)/shard_map/reduce_scatter | solution.py:211
  151.2 3.6 %copy-start.1 = (bf16[32,16,4096]{2,1,0:T(8,128)(2,1)S(1)}, bf16[32,16,4096]{2,1,0:T(8,128)(2,1)}, u32[]{:S(2)}) copy-start(bf16[32,16,4096]{2,1,0:T(8,128)(2,1)} %all-gather.2.cloned.1.call-done) | copy-start | bytes 12582916
  157.3 3.5 %copy-start.8 = (f32[128,2]{0,1:T(2,128)S(1)}, f32[128,2]{0,1:T(2,128)}, u32[]{:S(2)}) copy-start(f32[128,2]{0,1:T(2,128)} %param.32) | copy-start | bytes 3076
  226.6 20.9 %all-to-all-start.4 = ((bf16[32,16,256]{2,1,0:T(8,128)(2,1)}), bf16[32,16,256]{2,1,0:T(8,128)(2,1)S(1)}, u32[]{:S(2)}, u32[]{:S(2)}) async-start(bf16[32,16,256]{2,1,0:T(8,128)(2,1)} %bitcast.141), calls=%async_computation.5 | async-start | bytes 524288 | tf_op jit(solution)/shard_map/all_to_all | solution.py:215
Sparse Core Ops, SparseCore 0:
  106.1 45.1 all-gather.1
  160.6 65.9 reduce-scatter.1
where the time goes:
time: 257 us
  waiting for transfers between devices  159 us (62%)
  starting transfers between devices  37 us (14%)
  blocking collectives  15.2 us (6%)
  between operations  13.9 us (5%)
  matrix products  12.5 us (5%)
  local copies, waits for them, and re-layouts  9.55 us (4%)
  other arithmetic  9.4 us (4%)
    reduce_scatter x1, waiting for transfers between devices, per_device(): lax.psum_scatter(down_part.astype(f32).astype(jnp.bfloat16), 'tp', scatte...  65.8 us
    all_gather x1, waiting for transfers between devices, per_device(): piece = lax.all_gather(arrived, 'tp', axis=2, tiled=True)  45.2 us
    all_to_all x1, waiting for transfers between devices, sent_and_summed(): lax.all_to_all(in_blocks(array, dim, length), axis, 0, 0, tiled=True)  24.5 us
    all_to_all x2, starting transfers between devices, copy_for_each(): return lax.all_to_all(copies, axis, split_axis=0, concat_axis=0, tiled=True)  18.1 us
    all_to_all x1, blocking collectives, per_device(): lax.all_to_all(dispatch, 'sp', split_axis=0, concat_axis=0, tiled=True)  15.2 us
    all_to_all x2, waiting for transfers between devices, copy_for_each(): return lax.all_to_all(copies, axis, split_axis=0, concat_axis=0, tiled=True)  12.5 us
    all_to_all x1, waiting for transfers between devices, per_device(): lax.all_to_all(expert_out, 'sp', split_axis=0, concat_axis=0, tiled=True)  11 us
    all_to_all x1, starting transfers between devices, per_device(): lax.all_to_all(expert_out, 'sp', split_axis=0, concat_axis=0, tiled=True)  9.71 us
  transfers between devices with their start and end apart: 6, of which 6 were waited for; matrix products, arithmetic and copies ran while one was open for 1% of the time, Pallas kernels for 0%

commit v1 on v0

--- a/solution.py
+++ b/solution.py
@@ -202,7 +202,15 @@
         experts, capacity, d_local
     )
     arrived = lax.all_to_all(dispatch, "sp", split_axis=0, concat_axis=0, tiled=True)
-    piece = lax.all_gather(arrived, "tp", axis=2, tiled=True)
+    piece = jnp.concatenate(
+        lax.all_to_all(
+            jnp.stack(lax.axis_size("tp") * [arrived], axis=0),
+            axis_name="tp",
+            split_axis=0,
+            concat_axis=0,
+        ),
+        2,
+    )
     gate_part = jnp.einsum("snd,df->snf", piece, gate_w, preferred_element_type=f32)
     up_part = jnp.einsum("snd,df->snf", piece, up_w, preferred_element_type=f32)
     hidden = (jax.nn.silu(gate_part) * up_part).astype(bf16)

time: 257 us -> 304 us (1.18)
  blocking collectives: 15.2 us -> 116 us
  waiting for transfers between devices: 159 us -> 107 us
  matrix products: 12.5 us -> 8.95 us
    all_to_all x0 -> x1, blocking collectives: none -> 101 us  [per_device(): lax.all_to_all(jnp.stack(lax.axis_size('tp') * [arrived], axis=0), axis_n...]
    all_gather x1 -> x0, waiting for transfers between devices: 45.2 us -> none  [per_device(): piece = lax.all_gather(arrived, 'tp', axis=2, tiled=True)]
    reduce_scatter x1, waiting for transfers between devices: 65.8 us -> 58.8 us  [per_device(): lax.psum_scatter(down_part.astype(f32).astype(jnp.bfloat16), 'tp', scatte...]
  transfers between devices with their start and end apart: 6 -> 5, of which waited for: 6 -> 5; matrix products, arithmetic and copies ran while one was open for 1% -> 1% of each run, Pallas kernels for 0% -> 0%
where the time goes in v1:
time: 304 us; the launch traced here: 303 us
  blocking collectives  116 us (38%)
  waiting for transfers between devices  107 us (35%)
  starting transfers between devices  37 us (12%)
  between operations  13.9 us (5%)
  local copies, waits for them, and re-layouts  11.2 us (4%)
  other arithmetic  9.4 us (3%)
  matrix products  8.95 us (3%)
    all_to_all x1, blocking collectives, per_device(): lax.all_to_all(jnp.stack(lax.axis_size('tp') * [arrived], axis=0), axis_n...  101 us
    reduce_scatter x1, waiting for transfers between devices, per_device(): lax.psum_scatter(down_part.astype(f32).astype(jnp.bfloat16), 'tp', scatte...  58.8 us
    all_to_all x1, waiting for transfers between devices, sent_and_summed(): lax.all_to_all(in_blocks(array, dim, length), axis, 0, 0, tiled=True)  24.5 us
    all_to_all x2, starting transfers between devices, copy_for_each(): return lax.all_to_all(copies, axis, split_axis=0, concat_axis=0, tiled=True)  18.1 us
    all_to_all x1, blocking collectives, per_device(): lax.all_to_all(dispatch, 'sp', split_axis=0, concat_axis=0, tiled=True)  14.3 us
    all_to_all x2, waiting for transfers between devices, copy_for_each(): return lax.all_to_all(copies, axis, split_axis=0, concat_axis=0, tiled=True)  12.5 us
    all_to_all x1, waiting for transfers between devices, per_device(): lax.all_to_all(expert_out, 'sp', split_axis=0, concat_axis=0, tiled=True)  11 us
    all_to_all x1, starting transfers between devices, per_device(): lax.all_to_all(expert_out, 'sp', split_axis=0, concat_axis=0, tiled=True)  9.89 us
  transfers between devices with their start and end apart: 5, of which 5 were waited for; matrix products, arithmetic and copies ran while one was open for 1% of the time, Pallas kernels for 0%

profile of v1, /device:TPU:25, one launch (start us, length us, event | category | flops | bytes accessed | tf_op | source)
XLA Modules:
  0.0 303.0 jit_solution(1933098109671790382)
XLA Ops:
  6.5 0.7 exp.13
  7.3 0.8 fusion.57
  8.1 1.1 fusion.42
  9.2 1.1 fusion.46
  10.3 0.9 subtract_add_fusion.6
  11.2 1.0 add_add_fusion.5
  12.3 0.2 add_add_fusion.4
  12.7 0.2 add_add_fusion.3
  13.1 0.2 add_add_fusion.2
  13.4 0.2 add_add_fusion.1
  13.8 0.2 add_add_fusion
  14.0 0.2 multiply_subtract_fusion
  14.2 0.3 slice_reduce_fusion.1
  14.5 0.3 slice_reduce_fusion
  14.8 0.8 reshape.208
  15.6 12.9 %all-to-all-start = ((f32[32,1,1024]{2,1,0:T(1,128)}), f32[32,1,1024]{2,1,0:T(1,128)S(1)}, u32[]{:S(2)}, u32[]{:S(2)}) async-start(f32[32,1,1024]{2,1,0:T(1,128)} %reshape.208), calls=%async_computation | async-start | bytes 262144 | tf_op jit(solution)/shard_map/all_to_all | solution.py:12
  28.6 9.2 %all-to-all-done = f32[32,1,1024]{2,1,0:T(1,128)S(1)} async-done(((f32[32,1,1024]{2,1,0:T(1,128)}), f32[32,1,1024]{2,1,0:T(1,128)S(1)}, u32[]{:S(2)}, u32[]{:S(2)}) %all-to-all-start) | async-done | bytes 131104 | tf_op jit(solution)/shard_map/all_to_all | solution.py:12
  37.9 0.5 broadcast.193
  38.4 1.0 reduce.12
  39.8 0.3 fusion.16
  40.1 0.4 fusion.36
  40.5 0.5 convolution_convert_fusion.1
  41.0 1.1 copy.121
  42.1 9.0 %all-to-all-start.1 = ((bf16[16,128,256]{2,1,0:T(8,128)(2,1)}), bf16[16,128,256]{2,1,0:T(8,128)(2,1)S(1)}, u32[]{:S(2)}, u32[]{:S(2)}) async-start(bf16[16,128,256]{2,1,0:T(8,128)(2,1)} %bitcast.71), calls=%async_computation.1 | async-start | bytes 2097152 | tf_op jit(solution)/shard_map/all_to_all | solution.py:61
  51.5 0.6 reduce-window.6
  52.1 0.2 slice_reduce_fusion.4
  52.4 0.2 fusion.7
  52.8 24.5 %all-to-all-done.1 = bf16[16,128,256]{2,1,0:T(8,128)(2,1)S(1)} async-done(((bf16[16,128,256]{2,1,0:T(8,128)(2,1)}), bf16[16,128,256]{2,1,0:T(8,128)(2,1)S(1)}, u32[]{:S(2)}, u32[]{:S(2)}) %all-to-all-start.1) | async-done | bytes 1048608 | tf_op jit(solution)/shard_map/all_to_all | solution.py:61
  77.4 0.9 add_convert_fusion
  78.4 0.6 broadcast_in_dim.86
  79.0 5.2 %all-to-all-start.2 = ((f32[16,1,128]{2,1,0:T(1,128)}), f32[16,1,128]{2,1,0:T(1,128)S(1)}, u32[]{:S(2)}, u32[]{:S(2)}) async-start(f32[16,1,128]{2,1,0:T(1,128)} %broadcast_in_dim.86), calls=%async_computation.2 | async-start | bytes 16384 | tf_op jit(solution)/shard_map/all_to_all | solution.py:12
  84.3 0.8 dynamic_slice.7
  85.1 3.2 %all-to-all-done.2 = f32[16,1,128]{2,1,0:T(1,128)S(1)} async-done(((f32[16,1,128]{2,1,0:T(1,128)}), f32[16,1,128]{2,1,0:T(1,128)S(1)}, u32[]{:S(2)}, u32[]{:S(2)}) %all-to-all-start.2) | async-done | bytes 8224 | tf_op jit(solution)/shard_map/all_to_all | solution.py:12
  88.5 2.0 gather_fusion
  90.6 14.3 %all_to_all.31 = bf16[32,16,256]{2,1,0:T(8,128)(2,1)S(1)} all-to-all(bf16[32,16,256]{2,1,0:T(8,128)(2,1)S(1)} %broadcast_select_fusion), channel_id=1, replica_groups=mesh['sp'=32,'tp'=16] {'sp'}, dimensions={0} | all-to-all | bytes 524288 | tf_op jit(solution)/shard_map/all_to_all | solution.py:204
  104.9 0.4 stack.2
  105.4 101.4 %all_to_all.32 = bf16[16,32,16,256]{3,2,1,0:T(8,128)(2,1)S(1)} all-to-all(bf16[16,32,16,256]{3,2,1,0:T(8,128)(2,1)S(1)} %stack.2), channel_id=1, replica_groups=mesh['sp'=32,'tp'=16] {'tp'}, dimensions={0} | all-to-all | bytes 8388608 | tf_op jit(solution)/shard_map/all_to_all | solution.py:206
  206.8 0.5 copy.118
  207.4 0.7 copy-done.1
  208.0 1.2 fusion.5
  209.3 1.2 fusion
  210.6 3.2 %convolution_convert_fusion = bf16[512,4096]{1,0:T(8,128)(2,1)} fusion(bf16[512,128]{1,0:T(8,128)(2,1)S(1)} %bitcast.146, bf16[1,128,4096]{2,1,0:T(8,128)(2,1)S(1)} %copy-done), kind=kOutput, calls=%fused_computation.2 | convolution fusion | flops 538968064 | bytes 5373952 | tf_op jit(solution)/shard_map/dot_general | solution.py:218
  214.0 58.8 %reduce-scatter.2.cloned.1.call-done = bf16[512,256]{1,0:T(8,128)(2,1)} async-done(((bf16[512,4096]{1,0:T(8,128)(2,1)}), bf16[512,256]{1,0:T(8,128)(2,1)}) %reduce-scatter.2.cloned.1.call-update) | async-done | bytes 262160 | tf_op jit(solution)/shard_map/reduce_scatter | solution.py:219
  272.8 9.9 %all-to-all-start.5 = ((bf16[32,16,256]{2,1,0:T(8,128)(2,1)}), bf16[32,16,256]{2,1,0:T(8,128)(2,1)S(1)}, u32[]{:S(2)}, u32[]{:S(2)}) async-start(bf16[32,16,256]{2,1,0:T(8,128)(2,1)} %bitcast.147), calls=%async_computation.6 | async-start | bytes 524288 | tf_op jit(solution)/shard_map/all_to_all | solution.py:223
  282.9 11.0 %all-to-all-done.5 = bf16[32,16,256]{2,1,0:T(8,128)(2,1)S(1)} async-done(((bf16[32,16,256]{2,1,0:T(8,128)(2,1)}), bf16[32,16,256]{2,1,0:T(8,128)(2,1)S(1)}, u32[]{:S(2)}, u32[]{:S(2)}) %all-to-all-start.5) | async-done | bytes 262176 | tf_op jit(solution)/shard_map/all_to_all | solution.py:223
  293.9 1.2 gather_fusion.1
  295.1 0.4 multiply_reduce_fusion
  295.5 0.6 fusion.11
  (65 shorter events, 3.0 us)
Async XLA Ops:
  6.5 204.0 %copy-start = (bf16[1,128,4096]{2,1,0:T(8,128)(2,1)S(1)}, bf16[1,128,4096]{2,1,0:T(8,128)(2,1)}, u32[]{:S(2)}) copy-start(bf16[1,128,4096]{2,1,0:T(8,128)(2,1)} %param.35) | copy-start | bytes 3145732
  13.0 15.5 %copy-start.8 = (f32[64]{0:T(128)S(1)}, f32[64]{0:T(128)}, u32[]{:S(2)}) copy-start(f32[64]{0:T(128)} %param.26) | copy-start | bytes 772
  13.4 26.3 %copy-start.4 = (f32[4,16,64]{2,1,0:T(8,128)S(1)}, f32[4,16,64]{2,1,0:T(8,128)}, u32[]{:S(2)}) copy-start(f32[4,16,64]{2,1,0:T(8,128)} %param.24) | copy-start | bytes 49156
  13.4 26.7 %copy-start.3 = (bf16[64,128]{1,0:T(8,128)(2,1)S(1)}, bf16[64,128]{1,0:T(8,128)(2,1)}, u32[]{:S(2)}) copy-start(bf16[64,128]{1,0:T(8,128)(2,1)} %param.18) | copy-start | bytes 49156
  13.4 26.7 %copy-start.5 = (f32[4,16,64]{2,1,0:T(8,128)S(1)}, f32[4,16,64]{2,1,0:T(8,128)}, u32[]{:S(2)}) copy-start(f32[4,16,64]{2,1,0:T(8,128)} %param.25) | copy-start | bytes 49156
  13.7 26.8 %copy-start.2 = (bf16[64,4096]{1,0:T(8,128)(2,1)S(1)}, bf16[64,4096]{1,0:T(8,128)(2,1)}, u32[]{:S(2)}) copy-start(bf16[64,4096]{1,0:T(8,128)(2,1)} %param.28) | copy-start | bytes 1572868
  15.6 22.2 %all-to-all-start = ((f32[32,1,1024]{2,1,0:T(1,128)}), f32[32,1,1024]{2,1,0:T(1,128)S(1)}, u32[]{:S(2)}, u32[]{:S(2)}) async-start(f32[32,1,1024]{2,1,0:T(1,128)} %reshape.208), calls=%async_computation | async-start | bytes 262144 | tf_op jit(solution)/shard_map/all_to_all | solution.py:12
  39.4 11.7 %copy-start.6 = (s32[128,2]{0,1:T(2,128)S(1)}, s32[128,2]{0,1:T(2,128)}, u32[]{:S(2)}) copy-start(s32[128,2]{0,1:T(2,128)} %param.31) | copy-start | bytes 3076
  42.1 35.2 %all-to-all-start.1 = ((bf16[16,128,256]{2,1,0:T(8,128)(2,1)}), bf16[16,128,256]{2,1,0:T(8,128)(2,1)S(1)}, u32[]{:S(2)}, u32[]{:S(2)}) async-start(bf16[16,128,256]{2,1,0:T(8,128)(2,1)} %bitcast.71), calls=%async_computation.1 | async-start | bytes 2097152 | tf_op jit(solution)/shard_map/all_to_all | solution.py:61
  79.0 9.3 %all-to-all-start.2 = ((f32[16,1,128]{2,1,0:T(1,128)}), f32[16,1,128]{2,1,0:T(1,128)S(1)}, u32[]{:S(2)}, u32[]{:S(2)}) async-start(f32[16,1,128]{2,1,0:T(1,128)} %broadcast_in_dim.86), calls=%async_computation.2 | async-start | bytes 16384 | tf_op jit(solution)/shard_map/all_to_all | solution.py:12
  84.2 188.6 %reduce-scatter.2.cloned.1.call-start = ((), (), s32[]{:S(2)}) async-start(), calls=%async_computation.7 | async-start | bytes 4456448 | tf_op jit(solution)/shard_map/reduce_scatter | solution.py:219
  206.8 1.2 copy-start.1
  207.3 1.9 copy-start.9
  210.5 3.5 %copy-start.7 = (f32[128,2]{0,1:T(2,128)S(1)}, f32[128,2]{0,1:T(2,128)}, u32[]{:S(2)}) copy-start(f32[128,2]{0,1:T(2,128)} %param.32) | copy-start | bytes 3076
  272.8 21.1 %all-to-all-start.5 = ((bf16[32,16,256]{2,1,0:T(8,128)(2,1)}), bf16[32,16,256]{2,1,0:T(8,128)(2,1)S(1)}, u32[]{:S(2)}, u32[]{:S(2)}) async-start(bf16[32,16,256]{2,1,0:T(8,128)(2,1)} %bitcast.147), calls=%async_computation.6 | async-start | bytes 524288 | tf_op jit(solution)/shard_map/all_to_all | solution.py:223
Sparse Core Ops, SparseCore 0:
  213.9 58.9 reduce-scatter.1
